TPU v7x, 32 devices: a whole 2x2x4 slice. The times are simulated.
32 devices in a mesh: sp: 8 (over z, x), tp: 4 (over y, core).
Axes of the slice: x: 2, y: 2, z: 4, core: 2. Of those that a mesh axis runs over, the one named last changes fastest.
Arguments:
- tokens: bfloat16 [2048, 2048], P('sp', 'tp'), may hold values from -6 to 6
- segments: int32 [2048], P('sp'), may hold values from 0 to 3, never falling along the last dimension, each value on 1 to 1024 neighbouring positions
- in_gain: float32 [2, 2048], replicated, may hold values from 0.1 to 1.9
- w_value: bfloat16 [2, 2048, 1024], P(None, 'sp', 'tp'), may hold values from -0.125 to 0.125
- w_gate: bfloat16 [2, 2048, 1024], P(None, 'sp', 'tp'), may hold values from -0.125 to 0.125
- conv_taps: float32 [2, 129, 1024], P(None, None, 'tp'), may hold values from -4 to 4, as said below
- norm_gain: float32 [2, 1024], P(None, 'tp'), may hold values from 0.1 to 1.9
- w_out: bfloat16 [2, 1024, 2048], P(None, 'tp', 'sp'), may hold values from -0.1875 to 0.1875
Outputs:
- mixed: bfloat16 [2048, 2048], P('sp', 'tp')
Inputs may be any that keep to these rules, and one draw needn't show every extreme that they name: `segments`: document numbers never fall along the sequence; each document has 1 to 1024 positions, one has exactly 1024. `conv_taps`: real-valued taps.
All inputs are finite; a program needn't handle non-finite values.
Results may differ from a plain program's by a relative error of at most 0.014.
Values may be sent and summed in bfloat16 or wider, within the bound.
A program may use at most 64 MiB of HBM per device.

v0:
```python
import functools

import jax
import jax.numpy as jnp
from jax import lax
from jax.experimental import pallas as pl
from jax.experimental.pallas import tpu as pltpu
from jax.sharding import PartitionSpec as P

EPSILON = 0.01
LANES = 128
PAIR = 2
RELAY_MOST = 8
F32 = jnp.float32
BF16 = jnp.bfloat16
MESH = pl.DeviceIdType.MESH


def remote(src, dst, send, recv, axis, index):
    return pltpu.make_async_remote_copy(
        src_ref=src,
        dst_ref=dst,
        send_sem=send,
        recv_sem=recv,
        device_id={axis: index},
        device_id_type=MESH,
    )


def kernel(
    cfg, tok, seg, gain_in, wv, wg, wo, taps, gain_norm, out,
    stream, normed, gvg, gout, xbuf, segw, conv, act, stat, part, first, pair, far, own,
    w_recv, w_send_z, w_send_x, tok_recv, tok_send, sib_send, seg_send, seg_recv,
    halo_send, halo_recv, stat_send, stat_recv, first_send, first_recv,
    far_send, far_recv, fin_recv, fin_send,
):
    n_sp, n_tp, layers, kw, gather = cfg
    fringe = (kw - 1) // 2
    rows, width = tok.shape
    tiles = xbuf.shape[1]
    chan = tiles * LANES
    line, half = n_sp // PAIR, n_tp // PAIR
    s, t = lax.axis_index("sp"), lax.axis_index("tp")
    z, x = s // PAIR, lax.rem(s, PAIR)
    h, c = t // PAIR, lax.rem(t, PAIR)
    x_next = z * PAIR + (1 - x)
    sib = h * PAIR + (1 - c)

    barrier = pltpu.get_barrier_semaphore()
    greeted = range(1, n_sp) if gather else (1, n_sp - 1)
    for d in greeted:
        pl.semaphore_signal(barrier, inc=1, device_id={"sp": lax.rem(s + d, n_sp)}, device_id_type=MESH)
    for d in range(1, n_tp):
        pl.semaphore_signal(barrier, inc=1, device_id={"tp": lax.rem(t + d, n_tp)}, device_id_type=MESH)
    pl.semaphore_wait(barrier, len(greeted) + n_tp - 1)

    sends = []

    def go(copy):
        copy.start()
        sends.append(copy)

    def slot(layer, mat, origin):
        return gout.at[layer, origin] if mat == 2 else gvg.at[layer, mat, origin]

    def local(layer, mat):
        return (wv, wg, wo)[mat].at[layer]

    def send_own(layer, mat):
        if not gather:
            return
        p = layer * 3 + mat
        for d in range(1, line):
            go(remote(local(layer, mat), slot(layer, mat, s), w_send_z.at[p, d], w_recv.at[p, s], "sp",
                      lax.rem(z + d, line) * PAIR + x))
        go(remote(local(layer, mat), slot(layer, mat, s), w_send_x.at[p, 0], w_recv.at[p, s], "sp", x_next))
        slot(layer, mat, s)[...] = local(layer, mat)[...]

    def arrived(layer, mat, origin):
        p = layer * 3 + mat
        remote(local(layer, mat), slot(layer, mat, origin), w_send_x.at[p, 0], w_recv.at[p, origin], "sp", x_next).wait_recv()

    def relay(layer, mat):
        if not gather:
            return
        p = layer * 3 + mat
        for d in range(1, line):
            origin = lax.rem(z + line - d, line) * PAIR + x
            arrived(layer, mat, origin)
            block = slot(layer, mat, origin)
            go(remote(block, block, w_send_x.at[p, d], w_recv.at[p, origin], "sp", x_next))

    def settle(layer, mat):
        if not gather:
            return
        for d in range(line):
            arrived(layer, mat, lax.rem(z + line - d, line) * PAIR + (1 - x))

    def both_sides(make, count):
        for i in range(count):
            @pl.when(s > 0)
            def _():
                make(i, 0).start()

            @pl.when(s < n_sp - 1)
            def _():
                make(i, 1).start()

    def both_wait(make, count):
        for i in range(count):
            @pl.when(s > 0)
            def _():
                make(i, 0).wait_send()
                make(i, 1).wait_recv()

            @pl.when(s < n_sp - 1)
            def _():
                make(i, 1).wait_send()
                make(i, 0).wait_recv()

    def seg_copy(i, side):
        src = segw.at[pl.ds(fringe, fringe)] if side == 0 else segw.at[pl.ds(rows, fringe)]
        dst = segw.at[pl.ds(fringe + rows, fringe)] if side == 0 else segw.at[pl.ds(0, fringe)]
        return remote(src, dst, seg_send.at[side], seg_recv.at[side], "sp",
                      jnp.maximum(s - 1, 0) if side == 0 else jnp.minimum(s + 1, n_sp - 1))

    def halo_copy(layer):
        def make(i, side):
            buf = xbuf.at[layer, i]
            src = buf.at[pl.ds(fringe, fringe)] if side == 0 else buf.at[pl.ds(rows, fringe)]
            dst = buf.at[pl.ds(fringe + rows, fringe)] if side == 0 else buf.at[pl.ds(0, fringe)]
            return remote(src, dst, halo_send.at[layer, i, side], halo_recv.at[layer, i, side], "sp",
                          jnp.maximum(s - 1, 0) if side == 0 else jnp.minimum(s + 1, n_sp - 1))
        return make

    segw[pl.ds(fringe, rows)] = seg[...]

    @pl.when(s == 0)
    def _():
        segw[pl.ds(0, fringe)] = jnp.full((fringe, LANES), -1, jnp.int32)
        for layer in range(layers):
            for i in range(tiles):
                xbuf[layer, i, pl.ds(0, fringe)] = jnp.zeros((fringe, LANES), F32)

    @pl.when(s == n_sp - 1)
    def _():
        segw[pl.ds(fringe + rows, fringe)] = jnp.full((fringe, LANES), -1, jnp.int32)
        for layer in range(layers):
            for i in range(tiles):
                xbuf[layer, i, pl.ds(fringe + rows, fringe)] = jnp.zeros((fringe, LANES), F32)

    both_sides(seg_copy, 1)
    for mat in range(2):
        send_own(0, mat)
    for d in range(1, half):
        go(remote(tok, stream.at[0, t], tok_send.at[d], tok_recv.at[t], "tp", lax.rem(h + d, half) * PAIR + c))
    go(remote(tok, stream.at[0, t], sib_send.at[0, 0], tok_recv.at[t], "tp", sib))
    stream[0, t] = tok[...]
    relay(0, 0)
    send_own(0, 2)
    for d in range(1, half):
        origin = lax.rem(h + half - d, half) * PAIR + c
        block = stream.at[0, origin]
        remote(tok, block, tok_send.at[d], tok_recv.at[origin], "tp", sib).wait_recv()
        go(remote(block, block, sib_send.at[0, d], tok_recv.at[origin], "tp", sib))
    relay(0, 1)
    for d in range(half):
        origin = lax.rem(h + half - d, half) * PAIR + (1 - c)
        remote(tok, stream.at[0, origin], sib_send.at[0, d], tok_recv.at[origin], "tp", sib).wait_recv()
    both_wait(seg_copy, 1)

    for layer in range(layers):
        last = layer == layers - 1

        def norm_step(i, _):
            at = pl.ds(pl.multiple_of(i * 32, 32), 32)
            total = jnp.zeros((32, 1), F32)
            for j in range(n_tp):
                v = stream[layer, j, at, :].astype(F32)
                total = total + jnp.sum(v * v, axis=-1, keepdims=True)
            scale = lax.rsqrt(total / (n_tp * width) + EPSILON)
            for j in range(n_tp):
                v = stream[layer, j, at, :].astype(F32)
                cut = slice(j * width, (j + 1) * width)
                normed[at, cut] = (v * scale * gain_in[layer : layer + 1, cut]).astype(BF16)
            return 0

        lax.fori_loop(0, rows // 32, norm_step, 0)
        settle(layer, 0)
        settle(layer, 1)

        def gate_step(i):
            at = pl.ds(i * fringe, fringe)
            a = normed[at, :]
            if gather:
                w_value = gvg[layer, 0].reshape(n_tp * width, chan)
                w_gate = gvg[layer, 1].reshape(n_tp * width, chan)
            else:
                w_value, w_gate = wv[layer], wg[layer]
            value = jnp.dot(a, w_value, preferred_element_type=F32)
            gate = jnp.dot(a, w_gate, preferred_element_type=F32)
            gated = (value * jax.nn.sigmoid(gate)).astype(BF16).astype(F32)
            to = pl.ds(fringe + i * fringe, fringe)
            for j in range(tiles):
                xbuf[layer, j, to, :] = gated[:, j * LANES : (j + 1) * LANES]

        chunks = rows // fringe
        halo = halo_copy(layer)
        gate_step(0)
        gate_step(chunks - 1)
        both_sides(halo, tiles)
        if not last:
            send_own(layer + 1, 0)
        for i in range(1, chunks - 1):
            gate_step(i)

        def conv_step(i, _):
            base = pl.multiple_of(i * 32, 32)
            here = segw[pl.ds(base + fringe, 32), :]
            acc = [jnp.zeros((32, LANES), F32) for _ in range(tiles)]
            for shift in range(8):
                reach = (kw - 1 - shift) // 8 * 8
                docs = segw[pl.ds(base + shift, 32 + reach), :]
                data = [xbuf[layer, j, pl.ds(base + shift, 32 + reach), :] for j in range(tiles)]
                for q in range(0, reach + 1, 8):
                    same, k = docs[q : q + 32] == here, q + shift
                    for j in range(tiles):
                        tap = taps[layer, k : k + 1, j * LANES : (j + 1) * LANES]
                        acc[j] = acc[j] + jnp.where(same, data[j][q : q + 32] * tap, 0.0)
            at = pl.ds(base, 32)
            total = sum(jnp.sum(a, axis=-1, keepdims=True) for a in acc)
            mean = total / chan
            square = sum(jnp.sum((a - mean) * (a - mean), axis=-1, keepdims=True) for a in acc)
            for j in range(tiles):
                conv[at, j * LANES : (j + 1) * LANES] = acc[j]
            lane = lax.broadcasted_iota(jnp.int32, (32, LANES), 1)
            part[at, :] = jnp.where(lane == 0, mean, square)
            return 0

        edge = fringe // 32
        lax.fori_loop(edge, rows // 32 - edge, conv_step, 0)
        relay(layer, 2)
        if not last:
            send_own(layer + 1, 1)
        both_wait(halo, tiles)
        lax.fori_loop(0, edge, conv_step, 0)
        lax.fori_loop(rows // 32 - edge, rows // 32, conv_step, 0)
        if not last:
            send_own(layer + 1, 2)

        stat[layer, t] = jnp.transpose(part[...])[:8]
        for d in range(1, n_tp):
            go(remote(stat.at[layer, t], stat.at[layer, t], stat_send.at[layer, d], stat_recv.at[layer, t], "tp", lax.rem(t + d, n_tp)))
        for d in range(1, n_tp):
            origin = lax.rem(t + n_tp - d, n_tp)
            remote(stat.at[layer, t], stat.at[layer, origin], stat_send.at[layer, d], stat_recv.at[layer, origin], "tp", origin).wait_recv()
        means = [stat[layer, j][0:1] for j in range(n_tp)]
        mean = sum(means) / n_tp
        spread = sum(stat[layer, j][1:2] + chan * (means[j] - mean) * (means[j] - mean) for j in range(n_tp))
        scale = lax.rsqrt(spread / (n_tp * chan) + EPSILON)
        row = lax.broadcasted_iota(jnp.int32, (LANES, rows), 0)
        part[...] = jnp.transpose(jnp.where(row == 0, mean, scale))

        def act_step(i, _):
            at = pl.ds(pl.multiple_of(i * 32, 32), 32)
            both = part[at, :]
            v = (conv[at, :] - both[:, 0:1]) * both[:, 1:2] * gain_norm[layer : layer + 1, :]
            act[at, :] = (v / (1.0 + jnp.exp(-v))).astype(BF16)
            return 0

        lax.fori_loop(0, rows // 32, act_step, 0)
        settle(layer, 2)

        blocks = gout if gather else wo
        cols = blocks.shape[-1]
        each = width // cols

        def project(target, put):
            for i in range(each):
                w = blocks[layer, target * each + i]
                put(slice(i * cols, (i + 1) * cols), jnp.dot(act[...], w, preferred_element_type=F32))

        for k in range(half):
            def put_first(cut, v, k=k):
                first[layer, 0, k, :, cut] = v.astype(BF16)

            project(k * PAIR + (1 - c), put_first)
            go(remote(first.at[layer, 0, k], first.at[layer, 1, k], first_send.at[layer, k], first_recv.at[layer, k], "tp", sib))
        if not last:
            relay(layer + 1, 0)
        for k in range(half):
            def put_own(cut, v, k=k):
                own[k, :, cut] = v

            project(k * PAIR + c, put_own)
        for d in range(half):
            k = lax.rem(h + half - 1 - d, half) if last else d
            remote(first.at[layer, 0, k], first.at[layer, 1, k], first_send.at[layer, k], first_recv.at[layer, k], "tp", sib).wait_recv()
            pair[layer, k] = (own[k] + first[layer, 1, k].astype(F32)).astype(BF16)
            if last:
                @pl.when(k != h)
                def _():
                    remote(pair.at[layer, k], far.at[layer, h, 0], fin_send.at[k], fin_recv.at[h], "tp", k * PAIR + c).start()
            else:
                for e in range(1, half):
                    go(remote(pair.at[layer, k], far.at[layer, h, k], far_send.at[layer, e, k], far_recv.at[layer, h, k], "tp",
                              lax.rem(h + e, half) * PAIR + c))
        if last:
            far[layer, h, 0] = pair[layer, h]
            for e in range(1, half):
                k = lax.rem(h + e, half)
                remote(pair.at[layer, k], far.at[layer, k, 0], fin_send.at[k], fin_recv.at[k], "tp", sib).wait()
            total = sum(far[layer, g, 0].astype(F32) for g in range(half))
            out[...] = (stream[layer, t].astype(F32) + total).astype(BF16)
        else:
            for k in range(half):
                far[layer, h, k] = pair[layer, k]
            relay(layer + 1, 1)
            for k in range(half):
                for e in range(1, half):
                    g = lax.rem(h + e, half)
                    remote(pair.at[layer, k], far.at[layer, g, k], far_send.at[layer, e, k], far_recv.at[layer, g, k], "tp", sib).wait_recv()
                total = sum(far[layer, g, k].astype(F32) for g in range(half))
                block = stream.at[layer + 1, k * PAIR + c]
                block[...] = (stream[layer, k * PAIR + c].astype(F32) + total).astype(BF16)
                go(remote(block, block, sib_send.at[layer + 1, k], far_recv.at[layer, half, k], "tp", sib))
            for k in range(half):
                block = stream.at[layer + 1, k * PAIR + (1 - c)]
                remote(block, block, sib_send.at[layer + 1, k], far_recv.at[layer, half, k], "tp", sib).wait_recv()

    for copy in sends:
        copy.wait_send()


def per_device(n_sp, n_tp, tokens, segments, in_gain, w_value, w_gate, conv_taps, norm_gain, w_out):
    layers, kw, chan = conv_taps.shape
    rows, width = tokens.shape
    gather = n_sp <= RELAY_MOST and n_sp % PAIR == 0
    if not gather:
        w_value = lax.all_gather(w_value, "sp", axis=1, tiled=True)
        w_gate = lax.all_gather(w_gate, "sp", axis=1, tiled=True)
        w_out = lax.all_gather(w_out, "sp", axis=2, tiled=True)
        w_out = w_out.reshape(layers, chan, n_tp, width).transpose(0, 2, 1, 3)
    held = (layers, 2, n_sp) + w_value.shape[1:] if gather else (1, 1, 1, 16, LANES)
    held_out = (layers, n_sp) + w_out.shape[1:] if gather else (1, 1, 16, LANES)
    tiles, half, fringe = chan // LANES, n_tp // PAIR, (kw - 1) // 2
    wide = rows + 2 * fringe
    dma = pltpu.SemaphoreType.DMA
    line = max(n_sp // PAIR, 1) if gather else 1
    held_sp = n_sp if gather else 1
    vmem = pl.BlockSpec(memory_space=pltpu.VMEM)
    return pl.pallas_call(
        functools.partial(kernel, (n_sp, n_tp, layers, kw, gather)),
        out_shape=jax.ShapeDtypeStruct((rows, width), BF16),
        in_specs=[vmem] * 8,
        out_specs=vmem,
        scratch_shapes=[
            pltpu.VMEM((layers, n_tp, rows, width), BF16),
            pltpu.VMEM((rows, n_tp * width), BF16),
            pltpu.VMEM(held, BF16),
            pltpu.VMEM(held_out, BF16),
            pltpu.VMEM((layers, tiles, wide, LANES), F32),
            pltpu.VMEM((wide, LANES), jnp.int32),
            pltpu.VMEM((rows, chan), F32),
            pltpu.VMEM((rows, chan), BF16),
            pltpu.VMEM((layers, n_tp, 8, rows), F32),
            pltpu.VMEM((rows, LANES), F32),
            pltpu.VMEM((layers, 2, half, rows, width), BF16),
            pltpu.VMEM((layers, half, rows, width), BF16),
            pltpu.VMEM((layers, half, half, rows, width), BF16),
            pltpu.VMEM((half, rows, width), F32),
            dma((layers * 3, held_sp)),
            dma((layers * 3, line)),
            dma((layers * 3, line)),
            dma((n_tp,)),
            dma((half,)),
            dma((layers, half)),
            dma((2,)),
            dma((2,)),
            dma((layers, tiles, 2)),
            dma((layers, tiles, 2)),
            dma((layers, n_tp)),
            dma((layers, n_tp)),
            dma((layers, half)),
            dma((layers, half)),
            dma((layers, half, half)),
            dma((layers, half + 1, half)),
            dma((half,)),
            dma((half,)),
        ],
        compiler_params=pltpu.CompilerParams(
            collective_id=0, has_side_effects=True, vmem_limit_bytes=60000 * 1024
        ),
    )(
        tokens,
        jnp.broadcast_to(segments[:, None], (rows, LANES)),
        in_gain,
        w_value,
        w_gate,
        w_out,
        conv_taps,
        norm_gain,
    )


def solution(mesh):
    in_specs = (
        P("sp", "tp"),
        P("sp"),
        P(),
        P(None, "sp", "tp"),
        P(None, "sp", "tp"),
        P(None, None, "tp"),
        P(None, "tp"),
        P(None, "tp", "sp"),
    )
    return jax.shard_map(
        functools.partial(per_device, mesh.shape["sp"], mesh.shape["tp"]),
        mesh=mesh,
        in_specs=in_specs,
        out_specs=P("sp", "tp"),
        check_vma=False,
    )
```

profile of v0, /device:TPU:0, one launch (start us, length us, event | category | flops | bytes accessed | tf_op | source)
XLA Modules:
  0.0 108.4 jit_solution(13137895790455107655)
XLA Ops:
  0.0 1.4 %broadcast_in_dim.2.seg = s32[256,128]{1,0:T(8,128)} broadcast(s32[256]{0:T(256)} %param.9), dimensions={0} | broadcast | bytes 132096 | tf_op jit(solution)/shard_map/broadcast_in_dim | solution.py:396
  1.4 1.7 %copy.9.taps = f32[2,129,256]{2,1,0:T(8,128)} copy(f32[2,129,256]{2,0,1:T(2,128)} %param.13) | data formatting | bytes 528384 | tf_op args[5]
  3.1 103.7 %shard_map.82 = bf16[256,512]{1,0:T(8,128)(2,1)} custom-call(bf16[256,512]{1,0:T(8,128)(2,1)} %tok.1, s32[256,128]{1,0:T(8,128)} %broadcast_in_dim.2.seg, f32[2,2048]{1,0:T(2,128)} %gain_in.1, bf16[2,256,256]{2,1,0:T(8,128)(2,1)} %wv.1, bf16[2,256,256]{2,1,0:T(8,128)(2,1)} %wg.1, bf16[2,256,256]{2,1,0:T(8,128)(2,1)} %wo.1, f32[2,129,256]{2,1,0:T(8,128)} %copy.9.taps, ...), custom_call_target="tpu_custom_call" | custom-call | tf_op jit(solution)/shard_map/pallas_call | solution.py:352
  106.8 1.7 %copy.11 = bf16[256,512]{1,0:T(8,128)(2,1)} copy(bf16[256,512]{1,0:T(8,128)(2,1)} %shard_map.82) | data formatting | bytes 524288
where the time goes:
time: 109 us; the launch traced here: 108 us
  Pallas kernels  104 us (95%)
  local copies, waits for them, and re-layouts  4.77 us (4%)
    pallas_call x1, Pallas kernels, per_device(): pl.pallas_call(functools.partial(kernel, (n_sp, n_tp, layers, kw, gather)...  104 us
    unnamed x2, local copies, waits for them, and re-layouts  3.34 us

commit v1 on v0

v1 whole, which is shorter than its diff:
```python
import functools

import jax
import jax.numpy as jnp
from jax import lax
from jax.experimental import pallas as pl
from jax.experimental.pallas import tpu as pltpu
from jax.sharding import PartitionSpec as P

EPSILON = 0.01
LANES = 128
PAIR = 2
RELAY_MOST = 8
DETOUR = {1: 1, 2: 2, 4: 1}
F32 = jnp.float32
BF16 = jnp.bfloat16
MESH = pl.DeviceIdType.MESH


def remote(src, dst, send, recv, device):
    return pltpu.make_async_remote_copy(
        src_ref=src, dst_ref=dst, send_sem=send, recv_sem=recv, device_id=device, device_id_type=MESH
    )


def guarded(cond, act):
    if cond is None:
        act()
    else:
        pl.when(cond)(act)


def kernel(
    cfg, tok, seg, gain_in_hbm, wv, wg, wo, taps_hbm, gain_norm_hbm, out,
    stream, normed, gv, go_w, vacc, gacc, gbf, halo, xbuf, segw, segraw, segn, conv, act, stat, part,
    first, pair, far, own, gain_in, gain_norm, taps,
    local_sem, w_recv, w_send, tok_recv, tok_send, sib_send, seg_send, seg_recv,
    halo_send, halo_recv, stat_send, stat_recv, first_send, first_recv, far_send, far_recv, back_recv,
):
    n_sp, n_tp, layers, kw, gather = cfg
    fringe = (kw - 1) // 2
    rows, width = tok.shape
    tiles = xbuf.shape[0]
    chan = tiles * LANES
    line, half = n_sp // PAIR, n_tp // PAIR
    s, t = lax.axis_index("sp"), lax.axis_index("tp")
    z, x = s // PAIR, lax.rem(s, PAIR)
    h, c = t // PAIR, lax.rem(t, PAIR)
    x_next = z * PAIR + (1 - x)
    sib = h * PAIR + (1 - c)
    mats = 3
    chunk = rows // 2
    depth = min(wv.shape[1], width)
    blocks_in = n_tp * width // depth
    cols = go_w.shape[-1]
    each = width // cols

    sends = []

    def go(copy, cond=None):
        guarded(cond, copy.start)
        sends.append((copy, cond))

    def place(block):
        return (block % PAIR) * line + block // PAIR if gather else block

    def slot(p, zo, xo):
        layer, mat = p // mats, p % mats
        pos = xo * line + zo
        if mat == 2:
            return go_w.at[layer, pos]
        return gv.at[layer, mat, pl.ds(pl.multiple_of(pos * depth, depth), depth)]

    local = []

    def fetch(src, dst):
        copy = pltpu.make_async_copy(src, dst, local_sem.at[len(local)])
        copy.start()
        local.append(copy)
        return copy

    own_copies = []
    for p in range(layers * mats):
        src = (wv, wg, wo)[p % mats].at[p // mats]
        if gather:
            dst = slot(p, z, x)
        else:
            dst = go_w.at[p // mats] if p % mats == 2 else gv.at[p // mats, p % mats]
        own_copies.append((src, dst))
    weight_in = [fetch(*own_copies[0]), fetch(*own_copies[1])]
    tok_in = fetch(tok, stream.at[0, t])
    seg_in = fetch(seg, segraw)
    weight_in += [fetch(*pair_) for pair_ in own_copies[2:]]
    rest_in = [fetch(gain_in_hbm, gain_in), fetch(gain_norm_hbm, gain_norm), fetch(taps_hbm, taps)]

    barrier = pltpu.get_barrier_semaphore()
    prev_s, next_s = jnp.maximum(s - 1, 0), jnp.minimum(s + 1, n_sp - 1)

    def greet(device, cond=None):
        guarded(cond, lambda: pl.semaphore_signal(barrier, inc=1, device_id=device, device_id_type=MESH))

    for d in range(1, n_tp):
        greet({"tp": lax.rem(t + d, n_tp)})
    peers = n_tp - 1
    greet({"sp": prev_s}, s > 0)
    greet({"sp": next_s}, s < n_sp - 1)
    peers = peers + jnp.where(s > 0, 1, 0) + jnp.where(s < n_sp - 1, 1, 0)
    if gather:
        up = {"sp": jnp.minimum(s + PAIR, n_sp - 1)}
        down = {"sp": jnp.maximum(s - PAIR, 0)}
        side = {"sp": x_next}
        greet(up, z < line - 1)
        greet(down, z > 0)
        greet(side)
        peers = peers + 1 + jnp.where(z < line - 1, 1, 0) + jnp.where(z > 0, 1, 0)
    pl.semaphore_wait(barrier, peers)

    def push(p, kind, zo, xo, device, cond):
        block = slot(p, zo, xo)
        go(remote(block, block, w_send.at[p, kind], w_recv.at[p, xo * line + zo], device), cond)

    def landed(p, zo, xo, cond):
        block = slot(p, zo, xo)
        guarded(cond, remote(block, block, w_send.at[p, 0], w_recv.at[p, xo * line + zo], {"sp": x_next}).wait_recv)

    def own_z(p):
        if gather:
            push(p, 0, z, x, up, z < line - 1)
            push(p, 1, z, x, down, z > 0)

    def own_x(p):
        if gather:
            push(p, 2, z, x, side, None)

    def relay(p, d):
        if not gather or d >= line:
            return
        for sign in (1, -1):
            zo = z - sign * d
            here = (zo >= 0) if sign > 0 else (zo < line)
            safe = jnp.clip(zo, 0, line - 1)
            landed(p, safe, x, here)
            k = 3 + (0 if sign > 0 else 1) + 4 * (d - 1)
            onward = (z < line - 1) if sign > 0 else (z > 0)
            push(p, k, safe, x, up if sign > 0 else down, jnp.logical_and(here, onward))
            cross = here
            if p in DETOUR:
                cross = jnp.logical_and(here, safe != DETOUR[p])
            push(p, k + 2, safe, x, side, cross)

    def detour(p, d):
        if not gather or p not in DETOUR or d >= line:
            return
        zo = DETOUR[p]
        k = 3 + 4 * (line - 1)
        if d == 0:
            landed(p, zo, 1 - x, z == zo)
            push(p, k, zo, 1 - x, up, jnp.logical_and(z == zo, z < line - 1))
            push(p, k + 1, zo, 1 - x, down, jnp.logical_and(z == zo, z > 0))
        else:
            landed(p, zo, 1 - x, jnp.logical_or(z == zo + d, z == zo - d))
            push(p, k + 2 * d, zo, 1 - x, up, jnp.logical_and(z == zo + d, z < line - 1))
            push(p, k + 2 * d + 1, zo, 1 - x, down, jnp.logical_and(z == zo - d, z > 0))

    def settle(p):
        if not gather:
            return
        for d in range(line):
            for sign in ((1,) if d == 0 else (1, -1)):
                zo = z - sign * d
                safe = jnp.clip(zo, 0, line - 1)
                cond = None if d == 0 else ((zo >= 0) if sign > 0 else (zo < line))
                if p in DETOUR:
                    differs = safe != DETOUR[p]
                    cond = differs if cond is None else jnp.logical_and(cond, differs)
                landed(p, safe, 1 - x, cond)

    weight_in[0].wait()
    own_z(0)
    own_x(0)
    weight_in[1].wait()
    own_z(1)
    own_x(1)
    tok_in.wait()
    for d in range(1, half):
        go(remote(stream.at[0, t], stream.at[0, t], tok_send.at[d], tok_recv.at[t], {"tp": lax.rem(h + d, half) * PAIR + c}))
    go(remote(stream.at[0, t], stream.at[0, t], sib_send.at[0, 0], tok_recv.at[t], {"tp": sib}))
    seg_in.wait()

    def seg_copy(side_):
        return remote(segraw, segn.at[side_], seg_send.at[side_], seg_recv.at[side_], {"sp": prev_s if side_ else next_s})

    go(seg_copy(0), s < n_sp - 1)
    go(seg_copy(1), s > 0)

    def column(row):
        return jnp.transpose(jnp.broadcast_to(row.astype(F32), (LANES, LANES)))

    for i in range(rows // LANES):
        segw[pl.ds(fringe + i * LANES, LANES), :] = column(segraw[i : i + 1, :])

    relay(0, 1)
    relay(1, 1)
    for copy in weight_in[2:] + rest_in:
        copy.wait()
    for d in range(1, half):
        origin = lax.rem(h + half - d, half) * PAIR + c
        block = stream.at[0, origin]
        remote(block, block, tok_send.at[d], tok_recv.at[origin], {"tp": sib}).wait_recv()
        go(remote(block, block, sib_send.at[0, d], tok_recv.at[origin], {"tp": sib}))
    relay(0, 2)
    relay(1, 2)
    detour(1, 0)
    for d in range(half):
        origin = lax.rem(h + half - d, half) * PAIR + (1 - c)
        block = stream.at[0, origin]
        remote(block, block, sib_send.at[0, 0], tok_recv.at[origin], {"tp": sib}).wait_recv()
    guarded(s > 0, seg_copy(0).wait_recv)
    guarded(s < n_sp - 1, seg_copy(1).wait_recv)

    @pl.when(s > 0)
    def _():
        segw[pl.ds(0, fringe), :] = column(segn[0, rows // LANES - 1 : rows // LANES, :])[LANES - fringe :]

    @pl.when(s == 0)
    def _():
        segw[pl.ds(0, fringe), :] = jnp.full((fringe, LANES), -1.0, F32)

    @pl.when(s < n_sp - 1)
    def _():
        segw[pl.ds(fringe + rows, fringe), :] = column(segn[1, 0:1, :])[:fringe]

    @pl.when(s == n_sp - 1)
    def _():
        segw[pl.ds(fringe + rows, fringe), :] = jnp.full((fringe, LANES), -1.0, F32)

    spans = ((fringe, chunk),), ((0, fringe), (rows - fringe, fringe))

    for layer in range(layers):
        last = layer == layers - 1
        base_p = layer * mats

        def norm_step(i, _):
            at = pl.ds(pl.multiple_of(i * 32, 32), 32)
            total = jnp.zeros((32, 1), F32)
            for j in range(n_tp):
                v = stream[layer, j, at, :].astype(F32)
                total = total + jnp.sum(v * v, axis=-1, keepdims=True)
            scale = lax.rsqrt(total / (n_tp * width) + EPSILON)
            for b in range(blocks_in):
                j, lo = b * depth // width, b * depth % width
                v = stream[layer, j, at, lo : lo + depth].astype(F32)
                gain = gain_in[layer : layer + 1, b * depth : (b + 1) * depth]
                to = place(b) * depth
                normed[at, to : to + depth] = (v * scale * gain).astype(BF16)
            return 0

        lax.fori_loop(0, rows // 32, norm_step, 0)
        if layer == 0:
            relay(0, 3)
            relay(1, 3)
            detour(1, 1)
            detour(1, 2)
            own_z(2)

        size = n_tp * width // 2
        near = pl.multiple_of(x * size, size) if gather else 0
        away = pl.multiple_of((1 - x) * size, size) if gather else size
        a = normed[:, pl.ds(near, size)]
        vacc[...] = jnp.dot(a, gv[layer, 0, pl.ds(near, size), :], preferred_element_type=F32)
        gacc[...] = jnp.dot(a, gv[layer, 1, pl.ds(near, size), :], preferred_element_type=F32)
        settle(base_p)
        settle(base_p + 1)
        a = normed[:, pl.ds(away, size)]
        vacc[...] += jnp.dot(a, gv[layer, 0, pl.ds(away, size), :], preferred_element_type=F32)
        gacc[...] += jnp.dot(a, gv[layer, 1, pl.ds(away, size), :], preferred_element_type=F32)

        def gate_step(i, _):
            at = pl.ds(pl.multiple_of(i * 32, 32), 32)
            gated = (vacc[at, :] * jax.nn.sigmoid(gacc[at, :])).astype(BF16)
            gbf[layer, at, :] = gated
            wide = gated.astype(F32)
            to = pl.ds(pl.multiple_of(fringe + i * 32, 32), 32)
            for j in range(tiles):
                xbuf[j, to, :] = wide[:, j * LANES : (j + 1) * LANES]
            return 0

        lax.fori_loop(0, rows // 32, gate_step, 0)

        def halo_copy(side_):
            lo = 0 if side_ else rows - fringe
            return remote(
                gbf.at[layer, pl.ds(lo, fringe)], halo.at[layer, side_], halo_send.at[layer, side_],
                halo_recv.at[layer, side_], {"sp": prev_s if side_ else next_s},
            )

        go(halo_copy(0), s < n_sp - 1)
        go(halo_copy(1), s > 0)
        if layer == 0:
            own_x(2)
            relay(2, 1)
        if not last:
            own_z(base_p + 3)

        def conv_span(start, put):
            base = pl.multiple_of(start, fringe)
            here = [segw[pl.ds(base + fringe + 8 * m, 8), :] for m in range(8)]
            acc = [[jnp.zeros((8, LANES), F32) for _ in range(tiles)] for _ in range(8)]
            for shift in range(8):
                most = (kw - 1 - shift) // 8
                for n in range(most + 8):
                    at = pl.ds(base + 8 * n + shift, 8)
                    docs = segw[at, :]
                    data = [xbuf[j, at, :] for j in range(tiles)]
                    for m in range(8):
                        if 0 <= n - m <= most:
                            k = 8 * (n - m) + shift
                            same = docs == here[m]
                            for j in range(tiles):
                                tap = taps[k, layer : layer + 1, j * LANES : (j + 1) * LANES]
                                acc[m][j] = acc[m][j] + jnp.where(same, data[j] * tap, 0.0)
            lane = lax.broadcasted_iota(jnp.int32, (8, LANES), 1)
            for m in range(8):
                mean = sum(jnp.sum(v, axis=-1, keepdims=True) for v in acc[m]) / chan
                square = sum(jnp.sum((v - mean) * (v - mean), axis=-1, keepdims=True) for v in acc[m])
                at = pl.ds(put + 8 * m, 8)
                for j in range(tiles):
                    conv[at, j * LANES : (j + 1) * LANES] = acc[m][j]
                part[at, :] = jnp.where(lane == 0, mean, square)

        def send_stats(q):
            stat[layer, q, t] = jnp.transpose(part[pl.ds(q * chunk, chunk), :])[:8]
            for d in range(1, n_tp):
                go(remote(stat.at[layer, q, t], stat.at[layer, q, t], stat_send.at[layer, q, d], stat_recv.at[layer, q, t],
                          {"tp": lax.rem(t + d, n_tp)}))

        def middle(i, _):
            conv_span(fringe + i * fringe, pl.multiple_of(i * fringe, fringe))
            return 0

        lax.fori_loop(0, chunk // fringe, middle, 0)
        send_stats(0)
        if layer == 0:
            relay(2, 2)
            relay(2, 3)
            detour(2, 0)
        for side_, cond in ((0, s > 0), (1, s < n_sp - 1)):
            guarded(cond, halo_copy(side_).wait_recv)
            to = 0 if side_ == 0 else fringe + rows

            @pl.when(cond)
            def _(side_=side_, to=to):
                wide = halo[layer, side_].astype(F32)
                for j in range(tiles):
                    xbuf[j, pl.ds(to, fringe), :] = wide[:, j * LANES : (j + 1) * LANES]

            @pl.when(jnp.logical_not(cond))
            def _(to=to):
                for j in range(tiles):
                    xbuf[j, pl.ds(to, fringe), :] = jnp.zeros((fringe, LANES), F32)

        def edge(i, _):
            conv_span(i * (rows - fringe), pl.multiple_of(chunk + i * fringe, fringe))
            return 0

        lax.fori_loop(0, 2, edge, 0)
        send_stats(1)
        if layer == 0:
            detour(2, 1)
            detour(2, 2)
        if not last:
            own_x(base_p + 3)
            relay(base_p + 3, 1)
            own_z(base_p + 4)

        def activate(q):
            for d in range(1, n_tp):
                origin = lax.rem(t + n_tp - d, n_tp)
                remote(stat.at[layer, q, t], stat.at[layer, q, origin], stat_send.at[layer, q, d],
                       stat_recv.at[layer, q, origin], {"tp": origin}).wait_recv()
            means = [stat[layer, q, j][0:1] for j in range(n_tp)]
            mean = sum(means) / n_tp
            spread = sum(stat[layer, q, j][1:2] + chan * (means[j] - mean) * (means[j] - mean) for j in range(n_tp))
            scale = lax.rsqrt(spread / (n_tp * chan) + EPSILON)
            row = lax.broadcasted_iota(jnp.int32, (LANES, chunk), 0)
            part[pl.ds(q * chunk, chunk), :] = jnp.transpose(jnp.where(row == 0, mean, scale))

            def act_step(i, _):
                at = pl.ds(pl.multiple_of(q * chunk + i * 32, 32), 32)
                both = part[at, :]
                v = (conv[at, :] - both[:, 0:1]) * both[:, 1:2] * gain_norm[layer : layer + 1, :]
                act[at, :] = (v / (1.0 + jnp.exp(-v))).astype(BF16)
                return 0

            lax.fori_loop(0, chunk // 32, act_step, 0)

        def project(q, target, put):
            for i in range(each):
                block = target * each + i
                pos = lax.rem(block, PAIR) * line + block // PAIR if gather else block
                w = go_w[layer, pos]
                put(slice(i * cols, (i + 1) * cols),
                    jnp.dot(act[pl.ds(q * chunk, chunk), :], w, preferred_element_type=F32))

        def first_copy(q, k):
            return remote(first.at[layer, q, 0, k], first.at[layer, q, 1, k], first_send.at[layer, q, k],
                          first_recv.at[layer, q, k], {"tp": sib})

        def far_copy(q, k, e):
            g = lax.rem(h + e, half)
            return remote(pair.at[layer, q, k], far.at[layer, q, h, k], far_send.at[layer, q, e, k],
                          far_recv.at[layer, q, h, k], {"tp": g * PAIR + c})

        def far_wait(q, k, e):
            g = lax.rem(h + e, half)
            remote(pair.at[layer, q, k], far.at[layer, q, g, k], far_send.at[layer, q, e, k],
                   far_recv.at[layer, q, g, k], {"tp": sib}).wait_recv()

        def last_copy(q, e):
            k = lax.rem(h + e, half)
            return remote(pair.at[layer, q, k], far.at[layer, q, h, 0], far_send.at[layer, q, e, 0],
                          far_recv.at[layer, q, h, 0], {"tp": k * PAIR + c})

        def scatter(q):
            for k in range(half):
                def put_first(cut, v, k=k):
                    first[layer, q, 0, k, :, cut] = v.astype(BF16)

                project(q, k * PAIR + (1 - c), put_first)
                go(first_copy(q, k))
            for k in range(half):
                def put_own(cut, v, k=k):
                    own[k, :, cut] = v

                project(q, k * PAIR + c, put_own)
            for k in range(half):
                first_copy(q, k).wait_recv()
                pair[layer, q, k] = (own[k] + first[layer, q, 1, k].astype(F32)).astype(BF16)
                if not last:
                    for e in range(1, half):
                        go(far_copy(q, k, e))
            if last:
                for e in range(1, half):
                    go(last_copy(q, e))

        def rows_of(q):
            at = 0
            for lo, count in spans[q]:
                yield slice(at, at + count), slice(lo, lo + count)
                at += count

        def gather_stream(q):
            for k in range(half):
                for e in range(1, half):
                    far_wait(q, k, e)
                far[layer, q, h, k] = pair[layer, q, k]
                for src, dst in rows_of(q):
                    total = sum(far[layer, q, g, k, src].astype(F32) for g in range(half))
                    mine = k * PAIR + c
                    stream[layer + 1, mine, dst] = (stream[layer, mine, dst].astype(F32) + total).astype(BF16)
                    i = 0 if dst.start == spans[q][0][0] else 1
                    block = stream.at[layer + 1, mine, dst]
                    go(remote(block, block, sib_send.at[layer, half + 3 * k + q + i], back_recv.at[layer, 3 * k + q + i], {"tp": sib}))

        def gather_wait(q):
            for k in range(half):
                for i, (_, dst) in enumerate(rows_of(q)):
                    block = stream.at[layer + 1, k * PAIR + (1 - c), dst]
                    remote(block, block, sib_send.at[0, 0], back_recv.at[layer, 3 * k + q + i], {"tp": sib}).wait_recv()

        activate(0)
        settle(base_p + 2)
        scatter(0)
        activate(1)
        scatter(1)
        if not last:
            relay(base_p + 3, 2)
            relay(base_p + 3, 3)
            relay(base_p + 4, 1)
            own_x(base_p + 4)
            gather_stream(0)
            relay(base_p + 4, 2)
            relay(base_p + 4, 3)
            detour(base_p + 4, 0)
            detour(base_p + 4, 1)
            detour(base_p + 4, 2)
            own_z(base_p + 5)
            own_x(base_p + 5)
            gather_stream(1)
            relay(base_p + 5, 1)
            relay(base_p + 5, 2)
            relay(base_p + 5, 3)
            gather_wait(0)
            gather_wait(1)
        else:
            for q in range(2):
                far[layer, q, h, 0] = pair[layer, q, h]
                for e in range(1, half):
                    k = lax.rem(h + e, half)
                    remote(pair.at[layer, q, k], far.at[layer, q, k, 0], far_send.at[layer, q, e, 0],
                           far_recv.at[layer, q, k, 0], {"tp": sib}).wait_recv()
                for src, dst in rows_of(q):
                    total = sum(far[layer, q, g, 0, src].astype(F32) for g in range(half))
                    out[dst] = (stream[layer, t, dst].astype(F32) + total).astype(BF16)

    for copy, cond in sends:
        guarded(cond, copy.wait_send)


def per_device(n_sp, n_tp, tokens, segments, in_gain, w_value, w_gate, conv_taps, norm_gain, w_out):
    layers, kw, chan = conv_taps.shape
    rows, width = tokens.shape
    gather = n_sp <= RELAY_MOST and n_sp % PAIR == 0
    if not gather:
        w_value = lax.all_gather(w_value, "sp", axis=1, tiled=True)
        w_gate = lax.all_gather(w_gate, "sp", axis=1, tiled=True)
        w_out = lax.all_gather(w_out, "sp", axis=2, tiled=True)
        w_out = w_out.reshape(layers, chan, n_tp, width).transpose(0, 2, 1, 3)
    held_out = (layers, n_sp) + w_out.shape[1:] if gather else w_out.shape
    tiles, half, fringe = chan // LANES, n_tp // PAIR, (kw - 1) // 2
    wide, chunk = rows + 2 * fringe, rows // 2
    dma = pltpu.SemaphoreType.DMA
    line = n_sp // PAIR
    held_sp = n_sp if gather else 1
    kinds = 3 + 4 * (line - 1) + 2 * line if gather else 1
    hbm = pl.BlockSpec(memory_space=pl.ANY)
    vmem = pl.BlockSpec(memory_space=pltpu.VMEM)
    return pl.pallas_call(
        functools.partial(kernel, (n_sp, n_tp, layers, kw, gather)),
        out_shape=jax.ShapeDtypeStruct((rows, width), BF16),
        in_specs=[hbm] * 8,
        out_specs=vmem,
        scratch_shapes=[
            pltpu.VMEM((layers, n_tp, rows, width), BF16),
            pltpu.VMEM((rows, n_tp * width), BF16),
            pltpu.VMEM((layers, 2, n_tp * width, chan), BF16),
            pltpu.VMEM(held_out, BF16),
            pltpu.VMEM((rows, chan), F32),
            pltpu.VMEM((rows, chan), F32),
            pltpu.VMEM((layers, rows, chan), BF16),
            pltpu.VMEM((layers, 2, fringe, chan), BF16),
            pltpu.VMEM((tiles, wide, LANES), F32),
            pltpu.VMEM((wide, LANES), F32),
            pltpu.VMEM((rows // LANES, LANES), jnp.int32),
            pltpu.VMEM((2, rows // LANES, LANES), jnp.int32),
            pltpu.VMEM((rows, chan), F32),
            pltpu.VMEM((rows, chan), BF16),
            pltpu.VMEM((layers, 2, n_tp, 8, chunk), F32),
            pltpu.VMEM((rows, LANES), F32),
            pltpu.VMEM((layers, 2, 2, half, chunk, width), BF16),
            pltpu.VMEM((layers, 2, half, chunk, width), BF16),
            pltpu.VMEM((layers, 2, half, half, chunk, width), BF16),
            pltpu.VMEM((half, chunk, width), F32),
            pltpu.VMEM(in_gain.shape, F32),
            pltpu.VMEM(norm_gain.shape, F32),
            pltpu.VMEM((kw, layers, chan), F32),
            dma((layers * 3 + 5,)),
            dma((layers * 3, held_sp)),
            dma((layers * 3, kinds)),
            dma((n_tp,)),
            dma((half,)),
            dma((layers, 4 * half)),
            dma((2,)),
            dma((2,)),
            dma((layers, 2)),
            dma((layers, 2)),
            dma((layers, 2, n_tp)),
            dma((layers, 2, n_tp)),
            dma((layers, 2, half)),
            dma((layers, 2, half)),
            dma((layers, 2, half, half)),
            dma((layers, 2, half, half)),
            dma((layers, 3 * half)),
        ],
        compiler_params=pltpu.CompilerParams(
            collective_id=0, has_side_effects=True, vmem_limit_bytes=60000 * 1024
        ),
    )(
        tokens,
        segments.reshape(rows // LANES, LANES),
        in_gain,
        w_value,
        w_gate,
        w_out,
        conv_taps.transpose(1, 0, 2),
        norm_gain,
    )


def solution(mesh):
    in_specs = (
        P("sp", "tp"),
        P("sp"),
        P(),
        P(None, "sp", "tp"),
        P(None, "sp", "tp"),
        P(None, None, "tp"),
        P(None, "tp"),
        P(None, "tp", "sp"),
    )
    return jax.shard_map(
        functools.partial(per_device, mesh.shape["sp"], mesh.shape["tp"]),
        mesh=mesh,
        in_specs=in_specs,
        out_specs=P("sp", "tp"),
        check_vma=False,
    )
```

time: 109 us -> 105 us (0.963)
  local copies, waits for them, and re-layouts: 4.77 us -> 1.67 us
    unnamed x2 -> x1, local copies, waits for them, and re-layouts: 3.34 us -> 1.67 us
    broadcast_in_dim x1 -> x0, local copies, waits for them, and re-layouts: 1.43 us -> none  [per_device(): jnp.broadcast_to(segments[:, None], (rows, LANES))]
where the time goes in v1:
time: 105 us
  Pallas kernels  103 us (98%)
  local copies, waits for them, and re-layouts  1.67 us (2%)
    pallas_call x1, Pallas kernels, per_device(): pl.pallas_call(functools.partial(kernel, (n_sp, n_tp, layers, kw, gather)...  103 us

profile of v1, /device:TPU:0, one launch (start us, length us, event | category | flops | bytes accessed | tf_op | source)
XLA Modules:
  0.0 104.7 jit_solution(16277185196284070931)
XLA Ops:
  0.0 103.0 %shard_map.82 = bf16[256,512]{1,0:T(8,128)(2,1)} custom-call(bf16[256,512]{1,0:T(8,128)(2,1)} %tok.1, s32[2,128]{1,0:T(2,128)} %bitcast.3, f32[2,2048]{1,0:T(2,128)} %gain_in_hbm.1, bf16[2,256,256]{2,1,0:T(8,128)(2,1)} %wv.1, bf16[2,256,256]{2,1,0:T(8,128)(2,1)} %wg.1, bf16[2,256,256]{2,1,0:T(8,128)(2,1)} %wo.1, f32[129,2,256]{2,1,0:T(2,128)} %bitcast.2, ...), custom_call_target="tpu_custom_call" | custom-call | tf_op jit(solution)/shard_map/pallas_call | solution.py:528
  103.0 1.7 %copy.10 = bf16[256,512]{1,0:T(8,128)(2,1)} copy(bf16[256,512]{1,0:T(8,128)(2,1)} %shard_map.82) | data formatting | bytes 524288

commit v2 on v1

--- a/solution.py
+++ b/solution.py
@@ -11,7 +11,22 @@
 LANES = 128
 PAIR = 2
 RELAY_MOST = 8
-DETOUR = {1: 1, 2: 2, 4: 1}
+CHAIN = (0, 1)
+DETOUR = {3: 2, 5: 1}
+PLAN = {
+    (0, 11): (("r", 2, 1), ("c", 2, 1), ("z", 3, 0), ("r", 2, 2),),
+    (0, 0): (("c", 2, 2),),
+    (0, 1): (("r", 2, 3), ("c", 2, 3),),
+    (0, 2): (("d", 3, 0), ("z", 4, 0),),
+    (0, 4): (("r", 3, 1), ("c", 3, 1), ("r", 3, 2),),
+    (0, 5): (("c", 3, 2), ("r", 3, 3), ("c", 3, 3), ("d", 3, 1),),
+    (0, 6): (("r", 4, 1), ("c", 4, 1), ("z", 5, 0),),
+    (0, 7): (("d", 3, 2), ("r", 4, 2), ("c", 4, 2), ("r", 4, 3), ("c", 4, 3),),
+    (1, 0): (("r", 5, 1), ("c", 5, 1), ("d", 5, 0),),
+    (1, 1): (("r", 5, 2), ("c", 5, 2),),
+    (1, 2): (("r", 5, 3), ("c", 5, 3), ("d", 5, 1),),
+    (1, 3): (("d", 5, 2),),
+}
 F32 = jnp.float32
 BF16 = jnp.bfloat16
 MESH = pl.DeviceIdType.MESH
@@ -34,8 +49,9 @@
     cfg, tok, seg, gain_in_hbm, wv, wg, wo, taps_hbm, gain_norm_hbm, out,
     stream, normed, gv, go_w, vacc, gacc, gbf, halo, xbuf, segw, segraw, segn, conv, act, stat, part,
     first, pair, far, own, gain_in, gain_norm, taps,
-    local_sem, w_recv, w_send, tok_recv, tok_send, sib_send, seg_send, seg_recv,
+    psend, precv, otok, scl, local_sem, w_recv, w_send, tok_recv, tok_send, sib_send, seg_send, seg_recv,
     halo_send, halo_recv, stat_send, stat_recv, first_send, first_recv, far_send, far_recv, back_recv,
+    cross_send, cross_recv, part_send, part_recv,
 ):
     n_sp, n_tp, layers, kw, gather = cfg
     fringe = (kw - 1) // 2
@@ -109,10 +125,15 @@
         up = {"sp": jnp.minimum(s + PAIR, n_sp - 1)}
         down = {"sp": jnp.maximum(s - PAIR, 0)}
         side = {"sp": x_next}
+        up2 = {"sp": jnp.minimum(s + 2 * PAIR, n_sp - 1)}
+        down2 = {"sp": jnp.maximum(s - 2 * PAIR, 0)}
         greet(up, z < line - 1)
         greet(down, z > 0)
+        greet(up2, z < line - 2)
+        greet(down2, z > 1)
         greet(side)
         peers = peers + 1 + jnp.where(z < line - 1, 1, 0) + jnp.where(z > 0, 1, 0)
+        peers = peers + jnp.where(z < line - 2, 1, 0) + jnp.where(z > 1, 1, 0)
     pl.semaphore_wait(barrier, peers)
 
     def push(p, kind, zo, xo, device, cond):
@@ -127,26 +148,37 @@
         if gather:
             push(p, 0, z, x, up, z < line - 1)
             push(p, 1, z, x, down, z > 0)
+            if p not in CHAIN:
+                k = 3 + 4 * (line - 1) + 2 * line
+                push(p, k, z, x, up2, z < line - 2)
+                push(p, k + 1, z, x, down2, z > 1)
 
     def own_x(p):
         if gather:
             push(p, 2, z, x, side, None)
 
-    def relay(p, d):
-        if not gather or d >= line:
-            return
-        for sign in (1, -1):
+    def sides(d):
+        for i, sign in enumerate((1, -1)):
             zo = z - sign * d
             here = (zo >= 0) if sign > 0 else (zo < line)
-            safe = jnp.clip(zo, 0, line - 1)
-            landed(p, safe, x, here)
-            k = 3 + (0 if sign > 0 else 1) + 4 * (d - 1)
+            yield i, sign, jnp.clip(zo, 0, line - 1), here
+
+    def relay(p, d):
+        if d >= line:
+            return
+        for i, sign, zo, here in sides(d):
+            landed(p, zo, x, here)
             onward = (z < line - 1) if sign > 0 else (z > 0)
-            push(p, k, safe, x, up if sign > 0 else down, jnp.logical_and(here, onward))
-            cross = here
+            if p in CHAIN or d > 1:
+                push(p, 3 + i + 4 * (d - 1), zo, x, up if sign > 0 else down, jnp.logical_and(here, onward))
+
+    def across(p, d):
+        if d >= line:
+            return
+        for i, sign, zo, here in sides(d):
             if p in DETOUR:
-                cross = jnp.logical_and(here, safe != DETOUR[p])
-            push(p, k + 2, safe, x, side, cross)
+                here = jnp.logical_and(here, zo != DETOUR[p])
+            push(p, 5 + i + 4 * (d - 1), zo, x, side, here)
 
     def detour(p, d):
         if not gather or p not in DETOUR or d >= line:
@@ -163,7 +195,7 @@
             push(p, k + 2 * d + 1, zo, 1 - x, down, jnp.logical_and(z == zo - d, z > 0))
 
     def settle(p):
-        if not gather:
+        if not gather or p in CHAIN:
             return
         for d in range(line):
             for sign in ((1,) if d == 0 else (1, -1)):
@@ -177,14 +209,15 @@
 
     weight_in[0].wait()
     own_z(0)
-    own_x(0)
     weight_in[1].wait()
     own_z(1)
-    own_x(1)
     tok_in.wait()
     for d in range(1, half):
         go(remote(stream.at[0, t], stream.at[0, t], tok_send.at[d], tok_recv.at[t], {"tp": lax.rem(h + d, half) * PAIR + c}))
     go(remote(stream.at[0, t], stream.at[0, t], sib_send.at[0, 0], tok_recv.at[t], {"tp": sib}))
+    if gather:
+        theirs = pl.ds(pl.multiple_of((1 - x) * depth, depth), depth)
+        go(remote(stream.at[0, t, :, theirs], otok.at[t], cross_send.at[0], cross_recv.at[t], side))
     seg_in.wait()
 
     def seg_copy(side_):
@@ -199,8 +232,9 @@
     for i in range(rows // LANES):
         segw[pl.ds(fringe + i * LANES, LANES), :] = column(segraw[i : i + 1, :])
 
-    relay(0, 1)
-    relay(1, 1)
+    if gather:
+        relay(0, 1)
+        relay(1, 1)
     for copy in weight_in[2:] + rest_in:
         copy.wait()
     for d in range(1, half):
@@ -208,9 +242,26 @@
         block = stream.at[0, origin]
         remote(block, block, tok_send.at[d], tok_recv.at[origin], {"tp": sib}).wait_recv()
         go(remote(block, block, sib_send.at[0, d], tok_recv.at[origin], {"tp": sib}))
-    relay(0, 2)
-    relay(1, 2)
-    detour(1, 0)
+    if gather:
+        block = otok.at[t]
+        remote(block, block, cross_send.at[0], cross_recv.at[t], side).wait_recv()
+        for d in range(1, half):
+            go(remote(block, block, cross_send.at[d], cross_recv.at[t], {"tp": lax.rem(h + d, half) * PAIR + c}))
+        go(remote(block, block, cross_send.at[half], cross_recv.at[t], {"tp": sib}))
+        for p in range(2, layers * mats):
+            own_x(p)
+        relay(0, 2)
+        relay(1, 2)
+        own_z(2)
+        for d in range(1, half):
+            origin = lax.rem(h + half - d, half) * PAIR + c
+            block = otok.at[origin]
+            remote(block, block, cross_send.at[0], cross_recv.at[origin], {"tp": sib}).wait_recv()
+            go(remote(block, block, cross_send.at[half + d], cross_recv.at[origin], {"tp": sib}))
+        for d in range(half):
+            origin = lax.rem(h + half - d, half) * PAIR + (1 - c)
+            block = otok.at[origin]
+            remote(block, block, cross_send.at[0], cross_recv.at[origin], {"tp": sib}).wait_recv()
     for d in range(half):
         origin = lax.rem(h + half - d, half) * PAIR + (1 - c)
         block = stream.at[0, origin]
@@ -233,6 +284,15 @@
     @pl.when(s == n_sp - 1)
     def _():
         segw[pl.ds(fringe + rows, fringe), :] = jnp.full((fringe, LANES), -1.0, F32)
+
+    def steps(*names):
+        for name in names:
+            act_, p, d = name
+            {"z": lambda: own_z(p), "x": lambda: own_x(p), "r": lambda: relay(p, d), "c": lambda: across(p, d), "d": lambda: detour(p, d)}[act_]()
+
+    def weigh(layer, point):
+        if gather and (layer, point) in PLAN:
+            steps(*PLAN[layer, point])
 
     spans = ((fringe, chunk),), ((0, fringe), (rows - fringe, fringe))
 
@@ -255,25 +315,61 @@
                 normed[at, to : to + depth] = (v * scale * gain).astype(BF16)
             return 0
 
-        lax.fori_loop(0, rows // 32, norm_step, 0)
-        if layer == 0:
+        size = n_tp * width // 2
+
+        def parity_step(i, _):
+            at = pl.ds(pl.multiple_of(i * 32, 32), 32)
+            total = jnp.zeros((32, 1), F32)
+            for j in range(n_tp):
+                v = stream[layer, j, at, :].astype(F32)
+                total = total + jnp.sum(v * v, axis=-1, keepdims=True)
+                gain = gain_in[layer : layer + 1, pl.ds(pl.multiple_of((2 * j + x) * depth, depth), depth)]
+                mine = stream[layer, j, at, pl.ds(pl.multiple_of(x * depth, depth), depth)].astype(F32)
+                normed[at, j * depth : (j + 1) * depth] = (mine * gain).astype(BF16)
+                other = otok[j, at, :].astype(F32)
+                normed[at, size + j * depth : size + (j + 1) * depth] = (other * gain).astype(BF16)
+            scl[at, :] = jnp.broadcast_to(lax.rsqrt(total / (n_tp * width) + EPSILON), (32, LANES))
+            return 0
+
+        if gather and layer == 0:
+            lax.fori_loop(0, rows // 32, parity_step, 0)
             relay(0, 3)
             relay(1, 3)
-            detour(1, 1)
-            detour(1, 2)
-            own_z(2)
-
-        size = n_tp * width // 2
-        near = pl.multiple_of(x * size, size) if gather else 0
-        away = pl.multiple_of((1 - x) * size, size) if gather else size
-        a = normed[:, pl.ds(near, size)]
-        vacc[...] = jnp.dot(a, gv[layer, 0, pl.ds(near, size), :], preferred_element_type=F32)
-        gacc[...] = jnp.dot(a, gv[layer, 1, pl.ds(near, size), :], preferred_element_type=F32)
-        settle(base_p)
-        settle(base_p + 1)
-        a = normed[:, pl.ds(away, size)]
-        vacc[...] += jnp.dot(a, gv[layer, 0, pl.ds(away, size), :], preferred_element_type=F32)
-        gacc[...] += jnp.dot(a, gv[layer, 1, pl.ds(away, size), :], preferred_element_type=F32)
+            near = pl.ds(pl.multiple_of(x * size, size), size)
+            for i in range(2):
+                at = slice(i * chunk, (i + 1) * chunk)
+                for m in range(2):
+                    psend[at, m * chan : (m + 1) * chan] = jnp.dot(
+                        normed[at, size:], gv[layer, m, near, :], preferred_element_type=F32
+                    ).astype(BF16)
+                go(remote(psend.at[at], precv.at[at], part_send.at[i], part_recv.at[i], side))
+            vacc[...] = jnp.dot(normed[:, :size], gv[layer, 0, near, :], preferred_element_type=F32)
+            gacc[...] = jnp.dot(normed[:, :size], gv[layer, 1, near, :], preferred_element_type=F32)
+            weigh(layer, 11)
+            for i in range(2):
+                at = slice(i * chunk, (i + 1) * chunk)
+                remote(psend.at[at], precv.at[at], part_send.at[i], part_recv.at[i], side).wait_recv()
+
+            def sum_step(i, _):
+                at = pl.ds(pl.multiple_of(i * 32, 32), 32)
+                scale = scl[at, 0:1]
+                vacc[at, :] = (vacc[at, :] + precv[at, :chan].astype(F32)) * scale
+                gacc[at, :] = (gacc[at, :] + precv[at, chan:].astype(F32)) * scale
+                return 0
+
+            lax.fori_loop(0, rows // 32, sum_step, 0)
+        else:
+            lax.fori_loop(0, rows // 32, norm_step, 0)
+            near = pl.ds(pl.multiple_of(x * size, size), size) if gather else pl.ds(0, size)
+            away = pl.ds(pl.multiple_of((1 - x) * size, size), size) if gather else pl.ds(size, size)
+            a = normed[:, near]
+            vacc[...] = jnp.dot(a, gv[layer, 0, near, :], preferred_element_type=F32)
+            gacc[...] = jnp.dot(a, gv[layer, 1, near, :], preferred_element_type=F32)
+            settle(base_p)
+            settle(base_p + 1)
+            a = normed[:, away]
+            vacc[...] += jnp.dot(a, gv[layer, 0, away, :], preferred_element_type=F32)
+            gacc[...] += jnp.dot(a, gv[layer, 1, away, :], preferred_element_type=F32)
 
         def gate_step(i, _):
             at = pl.ds(pl.multiple_of(i * 32, 32), 32)
@@ -296,14 +392,10 @@
 
         go(halo_copy(0), s < n_sp - 1)
         go(halo_copy(1), s > 0)
-        if layer == 0:
-            own_x(2)
-            relay(2, 1)
-        if not last:
-            own_z(base_p + 3)
+        weigh(layer, 0)
 
         def conv_span(start, put):
-            base = pl.multiple_of(start, fringe)
+            base = start
             here = [segw[pl.ds(base + fringe + 8 * m, 8), :] for m in range(8)]
             acc = [[jnp.zeros((8, LANES), F32) for _ in range(tiles)] for _ in range(8)]
             for shift in range(8):
@@ -334,16 +426,12 @@
                 go(remote(stat.at[layer, q, t], stat.at[layer, q, t], stat_send.at[layer, q, d], stat_recv.at[layer, q, t],
                           {"tp": lax.rem(t + d, n_tp)}))
 
-        def middle(i, _):
-            conv_span(fringe + i * fringe, pl.multiple_of(i * fringe, fringe))
-            return 0
-
-        lax.fori_loop(0, chunk // fringe, middle, 0)
+        for i in range(chunk // fringe):
+            conv_span(fringe + i * fringe, i * fringe)
+            if i == 0:
+                weigh(layer, 1)
         send_stats(0)
-        if layer == 0:
-            relay(2, 2)
-            relay(2, 3)
-            detour(2, 0)
+        weigh(layer, 2)
         for side_, cond in ((0, s > 0), (1, s < n_sp - 1)):
             guarded(cond, halo_copy(side_).wait_recv)
             to = 0 if side_ == 0 else fringe + rows
@@ -359,19 +447,12 @@
                 for j in range(tiles):
                     xbuf[j, pl.ds(to, fringe), :] = jnp.zeros((fringe, LANES), F32)
 
-        def edge(i, _):
-            conv_span(i * (rows - fringe), pl.multiple_of(chunk + i * fringe, fringe))
-            return 0
-
-        lax.fori_loop(0, 2, edge, 0)
+        for i in range(2):
+            conv_span(i * (rows - fringe), chunk + i * fringe)
+            if i == 0:
+                weigh(layer, 3)
         send_stats(1)
-        if layer == 0:
-            detour(2, 1)
-            detour(2, 2)
-        if not last:
-            own_x(base_p + 3)
-            relay(base_p + 3, 1)
-            own_z(base_p + 4)
+        weigh(layer, 4)
 
         def activate(q):
             for d in range(1, n_tp):
@@ -469,27 +550,18 @@
                     remote(block, block, sib_send.at[0, 0], back_recv.at[layer, 3 * k + q + i], {"tp": sib}).wait_recv()
 
         activate(0)
+        weigh(layer, 10)
         settle(base_p + 2)
         scatter(0)
+        weigh(layer, 5)
         activate(1)
         scatter(1)
+        weigh(layer, 6)
         if not last:
-            relay(base_p + 3, 2)
-            relay(base_p + 3, 3)
-            relay(base_p + 4, 1)
-            own_x(base_p + 4)
             gather_stream(0)
-            relay(base_p + 4, 2)
-            relay(base_p + 4, 3)
-            detour(base_p + 4, 0)
-            detour(base_p + 4, 1)
-            detour(base_p + 4, 2)
-            own_z(base_p + 5)
-            own_x(base_p + 5)
+            weigh(layer, 7)
             gather_stream(1)
-            relay(base_p + 5, 1)
-            relay(base_p + 5, 2)
-            relay(base_p + 5, 3)
+            weigh(layer, 8)
             gather_wait(0)
             gather_wait(1)
         else:
@@ -522,7 +594,7 @@
     dma = pltpu.SemaphoreType.DMA
     line = n_sp // PAIR
     held_sp = n_sp if gather else 1
-    kinds = 3 + 4 * (line - 1) + 2 * line if gather else 1
+    kinds = 5 + 4 * (line - 1) + 2 * line if gather else 1
     hbm = pl.BlockSpec(memory_space=pl.ANY)
     vmem = pl.BlockSpec(memory_space=pltpu.VMEM)
     return pl.pallas_call(
@@ -554,6 +626,10 @@
             pltpu.VMEM(in_gain.shape, F32),
             pltpu.VMEM(norm_gain.shape, F32),
             pltpu.VMEM((kw, layers, chan), F32),
+            pltpu.VMEM((rows, 2 * chan), BF16),
+            pltpu.VMEM((rows, 2 * chan), BF16),
+            pltpu.VMEM((n_tp, rows, n_tp * width // n_sp if gather else LANES), BF16),
+            pltpu.VMEM((rows, LANES), F32),
             dma((layers * 3 + 5,)),
             dma((layers * 3, held_sp)),
             dma((layers * 3, kinds)),
@@ -571,6 +647,10 @@
             dma((layers, 2, half, half)),
             dma((layers, 2, half, half)),
             dma((layers, 3 * half)),
+            dma((2 * half,)),
+            dma((n_tp,)),
+            dma((2,)),
+            dma((2,)),
         ],
         compiler_params=pltpu.CompilerParams(
             collective_id=0, has_side_effects=True, vmem_limit_bytes=60000 * 1024

time: 105 us -> 87.7 us (0.84)
  Pallas kernels: 103 us -> 85.8 us
    pallas_call x1, Pallas kernels: 103 us -> 85.8 us  [per_device(): pl.pallas_call(functools.partial(kernel, (n_sp, n_tp, layers, kw, gather)...]
where the time goes in v2:
time: 87.7 us; the launch traced here: 87.5 us
  Pallas kernels  85.8 us (98%)
  local copies, waits for them, and re-layouts  1.67 us (2%)
    pallas_call x1, Pallas kernels, per_device(): pl.pallas_call(functools.partial(kernel, (n_sp, n_tp, layers, kw, gather)...  85.8 us

profile of v2, /device:TPU:0, one launch (start us, length us, event | category | flops | bytes accessed | tf_op | source)
XLA Modules:
  0.0 87.5 jit_solution(8969259596594596693)
XLA Ops:
  0.0 85.8 %shard_map.82 = bf16[256,512]{1,0:T(8,128)(2,1)} custom-call(bf16[256,512]{1,0:T(8,128)(2,1)} %tok.1, s32[2,128]{1,0:T(2,128)} %bitcast.3, f32[2,2048]{1,0:T(2,128)} %gain_in_hbm.1, bf16[2,256,256]{2,1,0:T(8,128)(2,1)} %wv.1, bf16[2,256,256]{2,1,0:T(8,128)(2,1)} %wg.1, bf16[2,256,256]{2,1,0:T(8,128)(2,1)} %wo.1, f32[129,2,256]{2,1,0:T(2,128)} %bitcast.2, ...), custom_call_target="tpu_custom_call" | custom-call | tf_op jit(solution)/shard_map/pallas_call | solution.py:600
  85.8 1.7 %copy.10 = bf16[256,512]{1,0:T(8,128)(2,1)} copy(bf16[256,512]{1,0:T(8,128)(2,1)} %shard_map.82) | data formatting | bytes 524288

commit v3 on v2

--- a/solution.py
+++ b/solution.py
@@ -14,14 +14,12 @@
 CHAIN = (0, 1)
 DETOUR = {3: 2, 5: 1}
 PLAN = {
-    (0, 11): (("r", 2, 1), ("c", 2, 1), ("z", 3, 0), ("r", 2, 2),),
+    (0, 11): (("r", 2, 1), ("c", 2, 1), ("r", 2, 2), ("z", 3, 0),),
     (0, 0): (("c", 2, 2),),
-    (0, 1): (("r", 2, 3), ("c", 2, 3),),
-    (0, 2): (("d", 3, 0), ("z", 4, 0),),
-    (0, 4): (("r", 3, 1), ("c", 3, 1), ("r", 3, 2),),
-    (0, 5): (("c", 3, 2), ("r", 3, 3), ("c", 3, 3), ("d", 3, 1),),
-    (0, 6): (("r", 4, 1), ("c", 4, 1), ("z", 5, 0),),
-    (0, 7): (("d", 3, 2), ("r", 4, 2), ("c", 4, 2), ("r", 4, 3), ("c", 4, 3),),
+    (0, 2): (("r", 2, 3), ("c", 2, 3),),
+    (0, 3): (("d", 3, 0), ("r", 3, 1), ("c", 3, 1), ("r", 3, 2), ("c", 3, 2), ("z", 4, 0),),
+    (0, 6): (("r", 3, 3), ("c", 3, 3), ("d", 3, 1), ("r", 4, 1), ("c", 4, 1), ("d", 3, 2), ("r", 4, 2), ("c", 4, 2), ("z", 5, 0),),
+    (0, 7): (("r", 4, 3), ("c", 4, 3),),
     (1, 0): (("r", 5, 1), ("c", 5, 1), ("d", 5, 0),),
     (1, 1): (("r", 5, 2), ("c", 5, 2),),
     (1, 2): (("r", 5, 3), ("c", 5, 3), ("d", 5, 1),),
@@ -47,7 +45,7 @@
 
 def kernel(
     cfg, tok, seg, gain_in_hbm, wv, wg, wo, taps_hbm, gain_norm_hbm, out,
-    stream, normed, gv, go_w, vacc, gacc, gbf, halo, xbuf, segw, segraw, segn, conv, act, stat, part,
+    stream, normed, gv, go_w, vacc, gacc, gbf, halo, xbuf, segw, segraw, segn, conv, act, stat,
     first, pair, far, own, gain_in, gain_norm, taps,
     psend, precv, otok, scl, local_sem, w_recv, w_send, tok_recv, tok_send, sib_send, seg_send, seg_recv,
     halo_send, halo_recv, stat_send, stat_recv, first_send, first_recv, far_send, far_recv, back_recv,
@@ -357,9 +355,9 @@
                 gacc[at, :] = (gacc[at, :] + precv[at, chan:].astype(F32)) * scale
                 return 0
 
-            lax.fori_loop(0, rows // 32, sum_step, 0)
+            lax.fori_loop(0, rows // 32, sum_step, 0, unroll=4)
         else:
-            lax.fori_loop(0, rows // 32, norm_step, 0)
+            lax.fori_loop(0, rows // 32, norm_step, 0, unroll=4)
             near = pl.ds(pl.multiple_of(x * size, size), size) if gather else pl.ds(0, size)
             away = pl.ds(pl.multiple_of((1 - x) * size, size), size) if gather else pl.ds(size, size)
             a = normed[:, near]
@@ -381,7 +379,7 @@
                 xbuf[j, to, :] = wide[:, j * LANES : (j + 1) * LANES]
             return 0
 
-        lax.fori_loop(0, rows // 32, gate_step, 0)
+        lax.fori_loop(0, rows // 32, gate_step, 0, unroll=2)
 
         def halo_copy(side_):
             lo = 0 if side_ else rows - fringe
@@ -411,17 +409,16 @@
                             for j in range(tiles):
                                 tap = taps[k, layer : layer + 1, j * LANES : (j + 1) * LANES]
                                 acc[m][j] = acc[m][j] + jnp.where(same, data[j] * tap, 0.0)
-            lane = lax.broadcasted_iota(jnp.int32, (8, LANES), 1)
             for m in range(8):
-                mean = sum(jnp.sum(v, axis=-1, keepdims=True) for v in acc[m]) / chan
-                square = sum(jnp.sum((v - mean) * (v - mean), axis=-1, keepdims=True) for v in acc[m])
-                at = pl.ds(put + 8 * m, 8)
                 for j in range(tiles):
-                    conv[at, j * LANES : (j + 1) * LANES] = acc[m][j]
-                part[at, :] = jnp.where(lane == 0, mean, square)
+                    conv[pl.ds(put + 8 * m, 8), j * LANES : (j + 1) * LANES] = acc[m][j]
 
         def send_stats(q):
-            stat[layer, q, t] = jnp.transpose(part[pl.ds(q * chunk, chunk), :])[:8]
+            at = slice(q * chunk, (q + 1) * chunk)
+            mean = jnp.sum(conv[at, :], axis=-1, keepdims=True) / chan
+            square = jnp.sum((conv[at, :] - mean) * (conv[at, :] - mean), axis=-1, keepdims=True)
+            lane = lax.broadcasted_iota(jnp.int32, (chunk, LANES), 1)
+            stat[layer, q, t] = jnp.transpose(jnp.where(lane == 0, mean, square))[:8]
             for d in range(1, n_tp):
                 go(remote(stat.at[layer, q, t], stat.at[layer, q, t], stat_send.at[layer, q, d], stat_recv.at[layer, q, t],
                           {"tp": lax.rem(t + d, n_tp)}))
@@ -464,16 +461,12 @@
             spread = sum(stat[layer, q, j][1:2] + chan * (means[j] - mean) * (means[j] - mean) for j in range(n_tp))
             scale = lax.rsqrt(spread / (n_tp * chan) + EPSILON)
             row = lax.broadcasted_iota(jnp.int32, (LANES, chunk), 0)
-            part[pl.ds(q * chunk, chunk), :] = jnp.transpose(jnp.where(row == 0, mean, scale))
-
-            def act_step(i, _):
-                at = pl.ds(pl.multiple_of(q * chunk + i * 32, 32), 32)
-                both = part[at, :]
-                v = (conv[at, :] - both[:, 0:1]) * both[:, 1:2] * gain_norm[layer : layer + 1, :]
+            both = jnp.transpose(jnp.where(row == 0, mean, scale))
+            for i in range(chunk // fringe):
+                at = slice(q * chunk + i * fringe, q * chunk + (i + 1) * fringe)
+                cut = both[i * fringe : (i + 1) * fringe]
+                v = (conv[at, :] - cut[:, 0:1]) * cut[:, 1:2] * gain_norm[layer : layer + 1, :]
                 act[at, :] = (v / (1.0 + jnp.exp(-v))).astype(BF16)
-                return 0
-
-            lax.fori_loop(0, chunk // 32, act_step, 0)
 
         def project(q, target, put):
             for i in range(each):
@@ -503,26 +496,25 @@
                           far_recv.at[layer, q, h, 0], {"tp": k * PAIR + c})
 
         def scatter(q):
-            for k in range(half):
+            order = [lax.rem(h + 1 + i, half) for i in range(half)] if last else list(range(half))
+            for k in order:
                 def put_first(cut, v, k=k):
                     first[layer, q, 0, k, :, cut] = v.astype(BF16)
 
                 project(q, k * PAIR + (1 - c), put_first)
                 go(first_copy(q, k))
-            for k in range(half):
-                def put_own(cut, v, k=k):
-                    own[k, :, cut] = v
+            for i, k in enumerate(order):
+                def put_own(cut, v, i=i):
+                    own[i, :, cut] = v
 
                 project(q, k * PAIR + c, put_own)
-            for k in range(half):
                 first_copy(q, k).wait_recv()
-                pair[layer, q, k] = (own[k] + first[layer, q, 1, k].astype(F32)).astype(BF16)
+                pair[layer, q, k] = (own[i] + first[layer, q, 1, k].astype(F32)).astype(BF16)
                 if not last:
                     for e in range(1, half):
                         go(far_copy(q, k, e))
-            if last:
-                for e in range(1, half):
-                    go(last_copy(q, e))
+                elif i < half - 1:
+                    go(last_copy(q, i + 1))
 
         def rows_of(q):
             at = 0
@@ -618,7 +610,6 @@
             pltpu.VMEM((rows, chan), F32),
             pltpu.VMEM((rows, chan), BF16),
             pltpu.VMEM((layers, 2, n_tp, 8, chunk), F32),
-            pltpu.VMEM((rows, LANES), F32),
             pltpu.VMEM((layers, 2, 2, half, chunk, width), BF16),
             pltpu.VMEM((layers, 2, half, chunk, width), BF16),
             pltpu.VMEM((layers, 2, half, half, chunk, width), BF16),

time: 87.7 us -> 86.4 us (0.985)
  Pallas kernels: 85.8 us -> 84.6 us
    pallas_call x1, Pallas kernels: 85.8 us -> 84.6 us  [per_device(): pl.pallas_call(functools.partial(kernel, (n_sp, n_tp, layers, kw, gather)...]
where the time goes in v3:
time: 86.4 us; the launch traced here: 86.2 us
  Pallas kernels  84.6 us (98%)
  local copies, waits for them, and re-layouts  1.67 us (2%)
    pallas_call x1, Pallas kernels, per_device(): pl.pallas_call(functools.partial(kernel, (n_sp, n_tp, layers, kw, gather)...  84.6 us

profile of v3, /device:TPU:0, one launch (start us, length us, event | category | flops | bytes accessed | tf_op | source)
XLA Modules:
  0.0 86.2 jit_solution(713807002323450954)
XLA Ops:
  0.0 84.6 %shard_map.82 = bf16[256,512]{1,0:T(8,128)(2,1)} custom-call(bf16[256,512]{1,0:T(8,128)(2,1)} %tok.1, s32[2,128]{1,0:T(2,128)} %bitcast.3, f32[2,2048]{1,0:T(2,128)} %gain_in_hbm.1, bf16[2,256,256]{2,1,0:T(8,128)(2,1)} %wv.1, bf16[2,256,256]{2,1,0:T(8,128)(2,1)} %wg.1, bf16[2,256,256]{2,1,0:T(8,128)(2,1)} %wo.1, f32[129,2,256]{2,1,0:T(2,128)} %bitcast.2, ...), custom_call_target="tpu_custom_call" | custom-call | tf_op jit(solution)/shard_map/pallas_call | solution.py:592
  84.6 1.7 %copy.10 = bf16[256,512]{1,0:T(8,128)(2,1)} copy(bf16[256,512]{1,0:T(8,128)(2,1)} %shard_map.82) | data formatting | bytes 524288
